TPU v7x, 32 devices: a whole 2x2x4 slice. The times are simulated.
32 devices in a mesh: fs: 4 (over z), tp: 8 (over y, x, core).
Axes of the slice: x: 2, y: 2, z: 4, core: 2. Of those that a mesh axis runs over, the one named last changes fastest.
Arguments:
- grad_gate: float32 [2112, 5632], P('fs', 'tp'), may hold values from -45 to 45
- grad_up: float32 [2112, 5632], P('fs', 'tp'), may hold values from -45 to 45
- moment_gate: float32 [2112, 5632], P('fs', 'tp'), may hold values from -6 to 6
- moment_up: float32 [2112, 5632], P('fs', 'tp'), may hold values from -6 to 6
Outputs:
- moment_gate_next: float32 [2112, 5632], P('fs', 'tp')
- moment_up_next: float32 [2112, 5632], P('fs', 'tp')
- update_gate: float32 [2112, 5632], P('fs', 'tp')
- update_up: float32 [2112, 5632], P('fs', 'tp')
All inputs are finite; a program needn't handle non-finite values.
Results may differ from a plain program's by a relative error of at most 0.0019.
The roundings to bfloat16 on the way count: a program that leaves them out, or rounds other values in their place, can miss the bound.
Values may be sent and summed in bfloat16 or wider, within the bound.
A program may use at most 64 MiB of HBM per device.

v0:
```python
import jax
import jax.numpy as jnp
from jax import lax
from jax.sharding import PartitionSpec as P

FF = 5632
ITERS = 3
BETA = 0.95
EPS = 1e-06


def multiply(left_low, right_low):
    left_rows = lax.all_gather(left_low, "fs", axis=1, tiled=True)
    return jnp.dot(
        left_rows,
        lax.all_gather(right_low, "tp", axis=0, tiled=True),
        preferred_element_type=jnp.float32,
    )


def local(grad_gate, grad_up, moment_gate, moment_up):
    moment_gate_next = BETA * moment_gate + grad_gate
    moment_up_next = BETA * moment_up + grad_up
    low_gate = moment_gate_next.astype(jnp.bfloat16)
    low_up = moment_up_next.astype(jnp.bfloat16)
    trace_local = jnp.sum(jnp.square(low_gate.astype(jnp.float32))) + jnp.sum(
        jnp.square(low_up.astype(jnp.float32))
    )
    columns_gate, columns_up = (
        lax.all_gather(low_gate, "fs", axis=0, tiled=True),
        lax.all_gather(low_up, "fs", axis=0, tiled=True),
    )
    rows_dev = low_gate.shape[0]
    width = columns_gate.shape[0]
    own_rows = width // lax.axis_size("tp")
    block_gate = columns_gate
    block_up = columns_up
    gram = lax.psum_scatter(
        jnp.einsum("ik,jk->ij", block_gate, low_gate, preferred_element_type=jnp.float32)
        + jnp.einsum("ik,jk->ij", block_up, low_up, preferred_element_type=jnp.float32),
        "tp",
        scatter_dimension=0,
        tiled=True,
    )
    square_local = jnp.sum(gram * gram)
    trace_total, square_total = lax.psum((trace_local, square_local), ("fs", "tp"))
    spectral = 2.0 * square_total / (trace_total + EPS)
    current = gram / spectral
    row_index = lax.axis_index("tp") * own_rows + lax.broadcasted_iota(
        jnp.int32, (own_rows, rows_dev), 0
    )
    col_index = lax.axis_index("fs") * rows_dev + lax.broadcasted_iota(
        jnp.int32, (own_rows, rows_dev), 1
    )
    identity = (row_index == col_index).astype(jnp.float32)
    product_low = None
    for iteration in range(ITERS):
        poly_low = (1.5 * identity - 0.5 * current).astype(jnp.bfloat16)
        final_turn = iteration == ITERS - 1
        square_low = None
        if iteration == 0:
            product_low = poly_low
            square_low = multiply(poly_low, poly_low).astype(jnp.bfloat16)
        elif final_turn:
            product_low = multiply(product_low, poly_low).astype(jnp.bfloat16)
        else:
            product_low = multiply(product_low, poly_low).astype(jnp.bfloat16)
            square_low = multiply(poly_low, poly_low).astype(jnp.bfloat16)
        if not final_turn:
            current = multiply(current.astype(jnp.bfloat16), square_low)
    factor = jnp.sqrt(2.0 * FF / spectral)
    segment = lax.all_gather(product_low, "tp", axis=0, tiled=True)
    block_gate = columns_gate
    block_up = columns_up
    ortho_gate = jnp.einsum("jr,jc->rc", segment, block_gate, preferred_element_type=jnp.float32)
    ortho_up = jnp.einsum("jr,jc->rc", segment, block_up, preferred_element_type=jnp.float32)
    return (moment_gate_next, moment_up_next, ortho_gate * factor, ortho_up * factor)


def solution(mesh):
    in_specs = (P("fs", "tp"), P("fs", "tp"), P("fs", "tp"), P("fs", "tp"))
    out_specs = (P("fs", "tp"), P("fs", "tp"), P("fs", "tp"), P("fs", "tp"))
    return jax.shard_map(local, mesh=mesh, in_specs=in_specs, out_specs=out_specs, check_vma=False)
```

profile of v0, /device:TPU:0, one launch (start us, length us, event | category | flops | bytes accessed | tf_op | source)
XLA Modules:
  0.0 640.1 jit_solution(17345301320345391013)
XLA Ops:
  7.2 4.4 multiply_reduce_fusion.1
  11.7 4.0 multiply_reduce_fusion
  15.8 63.8 %all-gather.19.cloned.1.call-done = bf16[2112,704]{1,0:T(8,128)(2,1)} async-done(((bf16[528,704]{1,0:T(8,128)(2,1)}), bf16[2112,704]{1,0:T(8,128)(2,1)}) %all-gather.19.cloned.1.call-update) | async-done | bytes 2973712 | tf_op jit(solution)/shard_map/all_gather | solution.py:30
  79.6 7.0 %fusion.5 = f32[2112,528]{1,0:T(8,128)} fusion(bf16[2112,704]{1,0:T(8,128)(2,1)} %all-gather.19.cloned.1.call-done, bf16[528,704]{1,0:T(8,128)(2,1)S(1)} %copy-done), kind=kOutput, calls=%fused_computation.25 | convolution fusion | flops 1570111488 | bytes 8177664 | tf_op jit(solution)/shard_map/ik,jk->ij/dot_general | solution.py:39
  86.6 58.9 %all-gather.21.cloned.1.call-done = bf16[2112,704]{1,0:T(8,128)(2,1)} async-done(((bf16[528,704]{1,0:T(8,128)(2,1)}), bf16[2112,704]{1,0:T(8,128)(2,1)}) %all-gather.21.cloned.1.call-update) | async-done | bytes 2973712 | tf_op jit(solution)/shard_map/all_gather | solution.py:31
  145.5 8.6 %convolution_add_fusion = f32[2112,528]{1,0:T(8,128)} fusion(f32[2112,528]{1,0:T(8,128)} %fusion.5, bf16[2112,704]{1,0:T(8,128)(2,1)} %all-gather.21.cloned.1.call-done, bf16[528,704]{1,0:T(8,128)(2,1)S(1)} %copy-done.1), kind=kOutput, calls=%fused_computation | convolution fusion | flops 1571226624 | bytes 12638208 | tf_op jit(solution)/shard_map/ik,jk->ij/dot_general | solution.py:40
  155.4 54.1 %reduce-scatter.4.cloned.1.call-done = f32[264,528]{1,0:T(8,128)} async-done(((f32[2112,528]{1,0:T(8,128)}), f32[264,528]{1,0:T(8,128)}) %reduce-scatter.4.cloned.1.call-update) | async-done | bytes 557584
  211.4 39.5 %all-reduce.1 = (f32[]{:T(128)}, f32[]{:T(128)}) all-reduce(f32[]{:T(128)} %multiply_reduce_fusion.2, f32[]{:T(128)S(6)} %add.42), channel_id=1, replica_groups=mesh['fs'=4,'tp'=8] {'fs','tp'}, use_global_device_ids=true, to_apply=%region_2.0 | all-reduce | flops 2 | bytes 16 | tf_op jit(solution)/shard_map/psum | solution.py:46
  255.6 33.1 %all-gather.35.cloned.1.call-done = bf16[4,528,264]{1,2,0:T(8,128)(2,1)} async-done(((bf16[1,528,264]{1,2,0:T(8,128)(2,1)}), bf16[4,528,264]{1,2,0:T(8,128)(2,1)}) %all-gather.35.cloned.1.call-update) | async-done | bytes 1115152 | tf_op jit(solution)/shard_map/all_gather | solution.py:13
  291.3 29.0 %all-gather.23.cloned.1.call-done = bf16[2112,528]{1,0:T(8,128)(2,1)} async-done(((bf16[264,528]{1,0:T(8,128)(2,1)}), bf16[2112,528]{1,0:T(8,128)(2,1)}) %all-gather.23.cloned.1.call-update) | async-done | bytes 2230288 | tf_op jit(solution)/shard_map/all_gather | solution.py:16
  324.2 31.4 %all-gather.37.cloned.1.call-done = bf16[4,528,264]{1,2,0:T(8,128)(2,1)} async-done(((bf16[1,528,264]{1,2,0:T(8,128)(2,1)}), bf16[4,528,264]{1,2,0:T(8,128)(2,1)}) %all-gather.37.cloned.1.call-update) | async-done | bytes 1115152 | tf_op jit(solution)/shard_map/all_gather | solution.py:13
  359.3 28.2 %all-gather.25.cloned.1.call-done = bf16[2112,528]{1,0:T(8,128)(2,1)} async-done(((bf16[264,528]{1,0:T(8,128)(2,1)}), bf16[2112,528]{1,0:T(8,128)(2,1)}) %all-gather.25.cloned.1.call-update) | async-done | bytes 2230288 | tf_op jit(solution)/shard_map/all_gather | solution.py:16
  387.5 4.1 convert_bitcast_fusion
  393.0 32.0 %all-gather.43.cloned.1.call-done = bf16[4,528,264]{1,2,0:T(8,128)(2,1)} async-done(((bf16[1,528,264]{1,2,0:T(8,128)(2,1)}), bf16[4,528,264]{1,2,0:T(8,128)(2,1)}) %all-gather.43.cloned.1.call-update) | async-done | bytes 1115152 | tf_op jit(solution)/shard_map/all_gather | solution.py:13
  428.7 27.6 %all-gather.27.cloned.1.call-done = bf16[2112,528]{1,0:T(8,128)(2,1)} async-done(((bf16[264,528]{1,0:T(8,128)(2,1)}), bf16[2112,528]{1,0:T(8,128)(2,1)}) %all-gather.27.cloned.1.call-update) | async-done | bytes 2230288 | tf_op jit(solution)/shard_map/all_gather | solution.py:16
  456.3 4.0 convolution_convert_fusion.1
  460.3 3.6 fusion.2
  464.0 27.5 %all-gather.41.cloned.1.call-done = bf16[4,528,264]{1,2,0:T(8,128)(2,1)} async-done(((bf16[1,528,264]{1,2,0:T(8,128)(2,1)}), bf16[4,528,264]{1,2,0:T(8,128)(2,1)}) %all-gather.41.cloned.1.call-update) | async-done | bytes 1115152 | tf_op jit(solution)/shard_map/all_gather | solution.py:13
  494.2 28.6 %all-gather.29.cloned.1.call-done = bf16[2112,528]{1,0:T(8,128)(2,1)} async-done(((bf16[264,528]{1,0:T(8,128)(2,1)}), bf16[2112,528]{1,0:T(8,128)(2,1)}) %all-gather.29.cloned.1.call-update) | async-done | bytes 2230288 | tf_op jit(solution)/shard_map/all_gather | solution.py:16
  522.9 3.6 fusion.1
  526.8 31.3 %all-gather.39.cloned.1.call-done = bf16[4,528,264]{1,2,0:T(8,128)(2,1)} async-done(((bf16[1,528,264]{1,2,0:T(8,128)(2,1)}), bf16[4,528,264]{1,2,0:T(8,128)(2,1)}) %all-gather.39.cloned.1.call-update) | async-done | bytes 1115152 | tf_op jit(solution)/shard_map/all_gather | solution.py:13
  560.8 29.2 %all-gather.31.cloned.1.call-done = bf16[2112,528]{1,0:T(8,128)(2,1)} async-done(((bf16[264,528]{1,0:T(8,128)(2,1)}), bf16[2112,528]{1,0:T(8,128)(2,1)}) %all-gather.31.cloned.1.call-update) | async-done | bytes 2230288 | tf_op jit(solution)/shard_map/all_gather | solution.py:16
  593.7 30.4 %all-gather.33.cloned.1.call-done = bf16[2112,528]{1,0:T(8,128)(2,1)} async-done(((bf16[264,528]{1,0:T(8,128)(2,1)}), bf16[2112,528]{1,0:T(8,128)(2,1)}) %all-gather.33.cloned.1.call-update) | async-done | bytes 2230288 | tf_op jit(solution)/shard_map/all_gather | solution.py:72
  624.1 6.1 convolution_multiply_fusion
  (55 shorter events, 33.3 us)
Async XLA Ops:
  7.2 72.4 %all-gather.19.cloned.1.call-start = ((), (), s32[]{:S(2)}) async-start(), calls=%async_computation.1 | async-start | bytes 4055040 | tf_op jit(solution)/shard_map/all_gather | solution.py:30
  7.2 4.5 copy-start.2
  11.7 67.9 %copy-start = (bf16[528,704]{1,0:T(8,128)(2,1)S(1)}, bf16[528,704]{1,0:T(8,128)(2,1)}, u32[]{:S(2)}) copy-start(bf16[528,704]{1,0:T(8,128)(2,1)} %get-tuple-element.10) | copy-start | bytes 2230276
  11.7 133.8 %all-gather.21.cloned.1.call-start = ((), (), s32[]{:S(2)}) async-start(), calls=%async_computation.2 | async-start | bytes 4055040 | tf_op jit(solution)/shard_map/all_gather | solution.py:31
  15.7 129.8 %copy-start.1 = (bf16[528,704]{1,0:T(8,128)(2,1)S(1)}, bf16[528,704]{1,0:T(8,128)(2,1)}, u32[]{:S(2)}) copy-start(bf16[528,704]{1,0:T(8,128)(2,1)} %get-tuple-element.7) | copy-start | bytes 2230276
  15.7 193.8 %reduce-scatter.4.cloned.1.call-start = ((), (), s32[]{:S(2)}) async-start(), calls=%async_computation.14 | async-start | bytes 6082560
  154.1 134.5 %all-gather.35.cloned.1.call-start = ((), (), s32[]{:S(2)}) async-start(), calls=%async_computation.9 | async-start | bytes 1689600 | tf_op jit(solution)/shard_map/all_gather | solution.py:13
  254.3 66.0 %all-gather.23.cloned.1.call-start = ((), (), s32[]{:S(2)}) async-start(), calls=%async_computation.3 | async-start | bytes 3041280 | tf_op jit(solution)/shard_map/all_gather | solution.py:16
  254.9 100.7 %all-gather.37.cloned.1.call-start = ((), (), s32[]{:S(2)}) async-start(), calls=%async_computation.10 | async-start | bytes 1689600 | tf_op jit(solution)/shard_map/all_gather | solution.py:13
  255.5 132.0 %all-gather.25.cloned.1.call-start = ((), (), s32[]{:S(2)}) async-start(), calls=%async_computation.4 | async-start | bytes 3041280 | tf_op jit(solution)/shard_map/all_gather | solution.py:16
  324.0 101.0 %all-gather.43.cloned.1.call-start = ((), (), s32[]{:S(2)}) async-start(), calls=%async_computation.13 | async-start | bytes 1689600 | tf_op jit(solution)/shard_map/all_gather | solution.py:13
  391.6 64.7 %all-gather.27.cloned.1.call-start = ((), (), s32[]{:S(2)}) async-start(), calls=%async_computation.5 | async-start | bytes 3041280 | tf_op jit(solution)/shard_map/all_gather | solution.py:16
  392.4 99.2 %all-gather.41.cloned.1.call-start = ((), (), s32[]{:S(2)}) async-start(), calls=%async_computation.12 | async-start | bytes 1689600 | tf_op jit(solution)/shard_map/all_gather | solution.py:13
  392.9 129.9 %all-gather.29.cloned.1.call-start = ((), (), s32[]{:S(2)}) async-start(), calls=%async_computation.6 | async-start | bytes 3041280 | tf_op jit(solution)/shard_map/all_gather | solution.py:16
  460.3 97.8 %all-gather.39.cloned.1.call-start = ((), (), s32[]{:S(2)}) async-start(), calls=%async_computation.11 | async-start | bytes 1689600 | tf_op jit(solution)/shard_map/all_gather | solution.py:13
  464.0 126.0 %all-gather.31.cloned.1.call-start = ((), (), s32[]{:S(2)}) async-start(), calls=%async_computation.7 | async-start | bytes 3041280 | tf_op jit(solution)/shard_map/all_gather | solution.py:16
  526.5 97.6 %all-gather.33.cloned.1.call-start = ((), (), s32[]{:S(2)}) async-start(), calls=%async_computation.8 | async-start | bytes 3041280 | tf_op jit(solution)/shard_map/all_gather | solution.py:72
  593.7 36.5 %copy-start.3 = (bf16[2112,704]{1,0:T(8,128)(2,1)S(1)}, bf16[2112,704]{1,0:T(8,128)(2,1)}, u32[]{:S(2)}) copy-start(bf16[2112,704]{1,0:T(8,128)(2,1)} %all-gather.19.cloned.1.call-done) | copy-start | bytes 8921092
  624.1 6.1 copy-start.4
Sparse Core Ops, SparseCore 0:
  11.8 67.7 all-gather.18
  81.7 63.6 all-gather.20
  154.2 55.2 reduce-scatter.3
  254.5 34.1 all-gather.34
  290.9 29.3 all-gather.22
  322.4 33.2 all-gather.36
  358.1 29.3 all-gather.24
  391.7 33.2 all-gather.42
  426.9 29.3 all-gather.26
  458.3 33.2 all-gather.40
  493.4 29.3 all-gather.28
  524.8 33.2 all-gather.38
  560.5 29.3 all-gather.30
  593.7 30.3 all-gather.32
where the time goes:
time: 641 us; the launch traced here: 640 us
  waiting for transfers between devices  508 us (79%)
  matrix products  47.6 us (7%)
  blocking collectives  39.5 us (6%)
  between operations  16.7 us (3%)
  local copies, waits for them, and re-layouts  15.4 us (2%)
  other arithmetic  12.4 us (2%)
    all_gather x5, waiting for transfers between devices, multiply(): left_rows = lax.all_gather(left_low, 'fs', axis=1, tiled=True)  155 us
    all_gather x5, waiting for transfers between devices, multiply(): lax.all_gather(right_low, 'tp', axis=0, tiled=True)  143 us
    all_gather x1, waiting for transfers between devices, local(): lax.all_gather(low_gate, 'fs', axis=0, tiled=True)  63.8 us
    all_gather x1, waiting for transfers between devices, local(): lax.all_gather(low_up, 'fs', axis=0, tiled=True)  58.9 us
    unnamed x15, waiting for transfers between devices  56.5 us
    psum x1, blocking collectives, local(): lax.psum((trace_local, square_local), ('fs', 'tp'))  39.5 us
    all_gather x1, waiting for transfers between devices, local(): segment = lax.all_gather(product_low, 'tp', axis=0, tiled=True)  30.4 us
    dot_general x6, matrix products, multiply(): jnp.dot(left_rows, lax.all_gather(right_low, 'tp', axis=0, tiled=True), p...  22.6 us
  transfers between devices with their start and end apart: 14, of which 14 were waited for; matrix products, arithmetic and copies ran while one was open for 6% of the time, Pallas kernels for 0%

commit v1 on v0

--- a/solution.py
+++ b/solution.py
@@ -9,8 +9,21 @@
 EPS = 1e-06
 
 
+def rest_wall_on_mesh(chunk, ax_name):
+    nd = jax.lax.axis_size(ax_name)
+    pile = [(tick, (tick + 1) % nd) for tick in range(nd)]
+
+    def close_waves(seen_now):
+        if len(seen_now) == nd:
+            return seen_now
+        return close_waves([jax.lax.ppermute(seen_now[0], ax_name, pile), *seen_now])
+
+    aux = jnp.concatenate(close_waves([chunk]), 1)
+    return jnp.roll(aux, (jax.lax.axis_index(ax_name) + 1) * chunk.shape[1], 1)
+
+
 def multiply(left_low, right_low):
-    left_rows = lax.all_gather(left_low, "fs", axis=1, tiled=True)
+    left_rows = rest_wall_on_mesh(left_low, "fs")
     return jnp.dot(
         left_rows,
         lax.all_gather(right_low, "tp", axis=0, tiled=True),

time: 641 us -> 480 us (0.75)
  waiting for transfers between devices: 508 us -> 347 us
    all_gather x5 -> x0, waiting for transfers between devices: 155 us -> none  [multiply(): left_rows = lax.all_gather(left_low, 'fs', axis=1, tiled=True)]
    all_gather x5, waiting for transfers between devices: 143 us -> 0.11 us  [multiply(): lax.all_gather(right_low, 'tp', axis=0, tiled=True)]
    ppermute x0 -> x15, waiting for transfers between devices: none -> 141 us  [close_waves(): jax.lax.ppermute(seen_now[0], ax_name, pile)]
    concatenate x0 -> x5, local copies, waits for them, and re-layouts: none -> 10.3 us  [rest_wall_on_mesh(): aux = jnp.concatenate(close_waves([chunk]), 1)]
    all_gather x5 -> x0, local copies, waits for them, and re-layouts: 9.26 us -> none  [multiply(): left_rows = lax.all_gather(left_low, 'fs', axis=1, tiled=True)]
    unnamed x15 -> x10, waiting for transfers between devices: 56.5 us -> 54.2 us
  transfers between devices with their start and end apart: 14 -> 24, of which waited for: 14 -> 19; matrix products, arithmetic and copies ran while one was open for 6% -> 5% of each run, Pallas kernels for 0% -> 0%
where the time goes in v1:
time: 480 us; the launch traced here: 479 us
  waiting for transfers between devices  347 us (72%)
  matrix products  51.1 us (11%)
  blocking collectives  39.5 us (8%)
  between operations  16.8 us (4%)
  other arithmetic  12.3 us (3%)
  local copies, waits for them, and re-layouts  10.3 us (2%)
    ppermute x15, waiting for transfers between devices, close_waves(): jax.lax.ppermute(seen_now[0], ax_name, pile)  141 us
    all_gather x1, waiting for transfers between devices, local(): lax.all_gather(low_gate, 'fs', axis=0, tiled=True)  63.8 us
    all_gather x1, waiting for transfers between devices, local(): lax.all_gather(low_up, 'fs', axis=0, tiled=True)  58.8 us
    unnamed x10, waiting for transfers between devices  54.2 us
    psum x1, blocking collectives, local(): lax.psum((trace_local, square_local), ('fs', 'tp'))  39.5 us
    all_gather x1, waiting for transfers between devices, local(): segment = lax.all_gather(product_low, 'tp', axis=0, tiled=True)  28.4 us
    dot_general x6, matrix products, multiply(): jnp.dot(left_rows, lax.all_gather(right_low, 'tp', axis=0, tiled=True), p...  26 us
    concatenate x5, local copies, waits for them, and re-layouts, rest_wall_on_mesh(): aux = jnp.concatenate(close_waves([chunk]), 1)  10.3 us
  transfers between devices with their start and end apart: 24, of which 19 were waited for; matrix products, arithmetic and copies ran while one was open for 5% of the time, Pallas kernels for 0%

profile of v1, /device:TPU:0, one launch (start us, length us, event | category | flops | bytes accessed | tf_op | source)
XLA Modules:
  0.0 479.0 jit_solution(15664307501275734671)
XLA Ops:
  15.8 63.8 %all-gather.9.cloned.1.call-done = bf16[2112,704]{1,0:T(8,128)(2,1)} async-done(((bf16[528,704]{1,0:T(8,128)(2,1)}), bf16[2112,704]{1,0:T(8,128)(2,1)}) %all-gather.9.cloned.1.call-update) | async-done | bytes 2973712 | tf_op jit(solution)/shard_map/all_gather | solution.py:43
  79.6 7.0 %fusion.26 = f32[2112,528]{1,0:T(8,128)} fusion(bf16[2112,704]{1,0:T(8,128)(2,1)} %all-gather.9.cloned.1.call-done, bf16[528,704]{1,0:T(8,128)(2,1)S(1)} %copy-done), kind=kOutput, calls=%fused_computation.48 | convolution fusion | flops 1570111488 | bytes 8177664 | tf_op jit(solution)/shard_map/ik,jk->ij/dot_general | solution.py:52
  86.7 58.8 %all-gather.11.cloned.1.call-done = bf16[2112,704]{1,0:T(8,128)(2,1)} async-done(((bf16[528,704]{1,0:T(8,128)(2,1)}), bf16[2112,704]{1,0:T(8,128)(2,1)}) %all-gather.11.cloned.1.call-update) | async-done | bytes 2973712 | tf_op jit(solution)/shard_map/all_gather | solution.py:44
  145.5 8.6 %convolution_add_fusion = f32[2112,528]{1,0:T(8,128)} fusion(f32[2112,528]{1,0:T(8,128)} %fusion.26, bf16[2112,704]{1,0:T(8,128)(2,1)} %all-gather.11.cloned.1.call-done, bf16[528,704]{1,0:T(8,128)(2,1)S(1)} %copy-done.1), kind=kOutput, calls=%fused_computation | convolution fusion | flops 1571226624 | bytes 12638208 | tf_op jit(solution)/shard_map/ik,jk->ij/dot_general | solution.py:53
  155.5 54.0 %reduce-scatter.4.cloned.1.call-done = f32[264,528]{1,0:T(8,128)} async-done(((f32[2112,528]{1,0:T(8,128)}), f32[264,528]{1,0:T(8,128)}) %reduce-scatter.4.cloned.1.call-update) | async-done | bytes 557584
  211.5 39.5 %all-reduce.1 = (f32[]{:T(128)}, f32[]{:T(128)}) all-reduce(f32[]{:T(128)} %multiply_reduce_fusion.2, f32[]{:T(128)S(6)} %add.58), channel_id=1, replica_groups=mesh['fs'=4,'tp'=8] {'fs','tp'}, use_global_device_ids=true, to_apply=%region_2.0 | all-reduce | flops 2 | bytes 16 | tf_op jit(solution)/shard_map/psum | solution.py:59
  255.9 9.6 %collective-permute-done = bf16[264,528]{1,0:T(8,128)(2,1)S(1)} collective-permute-done((bf16[264,528]{1,0:T(8,128)(2,1)}, bf16[264,528]{1,0:T(8,128)(2,1)S(1)}, u32[]{:S(2)}, u32[]{:S(2)}) %collective-permute-start) | collective-permute-done | bytes 278816 | tf_op jit(solution)/shard_map/ppermute | solution.py:19
  265.5 10.0 %collective-permute-done.1 = bf16[264,528]{1,0:T(8,128)(2,1)S(1)} collective-permute-done((bf16[264,528]{1,0:T(8,128)(2,1)S(1)}, bf16[264,528]{1,0:T(8,128)(2,1)S(1)}, u32[]{:S(2)}, u32[]{:S(2)}) %collective-permute-start.1) | collective-permute-done | bytes 278816 | tf_op jit(solution)/shard_map/ppermute | solution.py:19
  275.4 9.1 %collective-permute-done.2 = bf16[264,528]{1,0:T(8,128)(2,1)S(1)} collective-permute-done((bf16[264,528]{1,0:T(8,128)(2,1)S(1)}, bf16[264,528]{1,0:T(8,128)(2,1)S(1)}, u32[]{:S(2)}, u32[]{:S(2)}) %collective-permute-start.2) | collective-permute-done | bytes 278816 | tf_op jit(solution)/shard_map/ppermute | solution.py:19
  291.8 10.4 %collective-permute-done.3 = bf16[264,528]{1,0:T(8,128)(2,1)S(1)} collective-permute-done((bf16[264,528]{1,0:T(8,128)(2,1)S(1)}, bf16[264,528]{1,0:T(8,128)(2,1)S(1)}, u32[]{:S(2)}, u32[]{:S(2)}) %collective-permute-start.3) | collective-permute-done | bytes 278816 | tf_op jit(solution)/shard_map/ppermute | solution.py:19
  302.1 9.7 %collective-permute-done.4 = bf16[264,528]{1,0:T(8,128)(2,1)S(1)} collective-permute-done((bf16[264,528]{1,0:T(8,128)(2,1)S(1)}, bf16[264,528]{1,0:T(8,128)(2,1)S(1)}, u32[]{:S(2)}, u32[]{:S(2)}) %collective-permute-start.4) | collective-permute-done | bytes 278816 | tf_op jit(solution)/shard_map/ppermute | solution.py:19
  311.9 9.1 %collective-permute-done.5 = bf16[264,528]{1,0:T(8,128)(2,1)} collective-permute-done((bf16[264,528]{1,0:T(8,128)(2,1)S(1)}, bf16[264,528]{1,0:T(8,128)(2,1)}, u32[]{:S(2)}, u32[]{:S(2)}) %collective-permute-start.5) | collective-permute-done | bytes 278816 | tf_op jit(solution)/shard_map/ppermute | solution.py:19
  323.3 4.5 fusion.25
  327.9 9.4 %collective-permute-done.12 = bf16[264,528]{1,0:T(8,128)(2,1)S(1)} collective-permute-done((bf16[264,528]{1,0:T(8,128)(2,1)}, bf16[264,528]{1,0:T(8,128)(2,1)S(1)}, u32[]{:S(2)}, u32[]{:S(2)}) %collective-permute-start.12) | collective-permute-done | bytes 278816 | tf_op jit(solution)/shard_map/ppermute | solution.py:19
  337.3 9.0 %collective-permute-done.13 = bf16[264,528]{1,0:T(8,128)(2,1)S(1)} collective-permute-done((bf16[264,528]{1,0:T(8,128)(2,1)S(1)}, bf16[264,528]{1,0:T(8,128)(2,1)S(1)}, u32[]{:S(2)}, u32[]{:S(2)}) %collective-permute-start.13) | collective-permute-done | bytes 278816 | tf_op jit(solution)/shard_map/ppermute | solution.py:19
  346.3 9.1 %collective-permute-done.14 = bf16[264,528]{1,0:T(8,128)(2,1)} collective-permute-done((bf16[264,528]{1,0:T(8,128)(2,1)S(1)}, bf16[264,528]{1,0:T(8,128)(2,1)}, u32[]{:S(2)}, u32[]{:S(2)}) %collective-permute-start.14) | collective-permute-done | bytes 278816 | tf_op jit(solution)/shard_map/ppermute | solution.py:19
  362.4 10.1 %collective-permute-done.9 = bf16[264,528]{1,0:T(8,128)(2,1)S(1)} collective-permute-done((bf16[264,528]{1,0:T(8,128)(2,1)S(1)}, bf16[264,528]{1,0:T(8,128)(2,1)S(1)}, u32[]{:S(2)}, u32[]{:S(2)}) %collective-permute-start.9) | collective-permute-done | bytes 278816 | tf_op jit(solution)/shard_map/ppermute | solution.py:19
  372.5 9.2 %collective-permute-done.10 = bf16[264,528]{1,0:T(8,128)(2,1)S(1)} collective-permute-done((bf16[264,528]{1,0:T(8,128)(2,1)S(1)}, bf16[264,528]{1,0:T(8,128)(2,1)S(1)}, u32[]{:S(2)}, u32[]{:S(2)}) %collective-permute-start.10) | collective-permute-done | bytes 278816 | tf_op jit(solution)/shard_map/ppermute | solution.py:19
  381.7 9.1 %collective-permute-done.11 = bf16[264,528]{1,0:T(8,128)(2,1)} collective-permute-done((bf16[264,528]{1,0:T(8,128)(2,1)S(1)}, bf16[264,528]{1,0:T(8,128)(2,1)}, u32[]{:S(2)}, u32[]{:S(2)}) %collective-permute-start.11) | collective-permute-done | bytes 278816 | tf_op jit(solution)/shard_map/ppermute | solution.py:19
  401.4 9.7 %collective-permute-done.6 = bf16[264,528]{1,0:T(8,128)(2,1)S(1)} collective-permute-done((bf16[264,528]{1,0:T(8,128)(2,1)S(1)}, bf16[264,528]{1,0:T(8,128)(2,1)S(1)}, u32[]{:S(2)}, u32[]{:S(2)}) %collective-permute-start.6) | collective-permute-done | bytes 278816 | tf_op jit(solution)/shard_map/ppermute | solution.py:19
  411.1 9.1 %collective-permute-done.7 = bf16[264,528]{1,0:T(8,128)(2,1)S(1)} collective-permute-done((bf16[264,528]{1,0:T(8,128)(2,1)S(1)}, bf16[264,528]{1,0:T(8,128)(2,1)S(1)}, u32[]{:S(2)}, u32[]{:S(2)}) %collective-permute-start.7) | collective-permute-done | bytes 278816 | tf_op jit(solution)/shard_map/ppermute | solution.py:19
  420.2 9.0 %collective-permute-done.8 = bf16[264,528]{1,0:T(8,128)(2,1)S(1)} collective-permute-done((bf16[264,528]{1,0:T(8,128)(2,1)S(1)}, bf16[264,528]{1,0:T(8,128)(2,1)S(1)}, u32[]{:S(2)}, u32[]{:S(2)}) %collective-permute-start.8) | collective-permute-done | bytes 278816 | tf_op jit(solution)/shard_map/ppermute | solution.py:19
  434.7 28.4 %all-gather.23.cloned.1.call-done = bf16[2112,528]{1,0:T(8,128)(2,1)} async-done(((bf16[264,528]{1,0:T(8,128)(2,1)}), bf16[2112,528]{1,0:T(8,128)(2,1)}) %all-gather.23.cloned.1.call-update) | async-done | bytes 2230288 | tf_op jit(solution)/shard_map/all_gather | solution.py:85
  463.1 6.1 %convolution_multiply_fusion = f32[528,704]{1,0:T(8,128)} fusion(bf16[2112,528]{1,0:T(8,128)(2,1)} %all-gather.23.cloned.1.call-done, bf16[2112,704]{1,0:T(8,128)(2,1)} %all-gather.11.cloned.1.call-done, f32[]{:T(128)S(6)} %sqrt.3), kind=kOutput, calls=%fused_computation.15 | convolution fusion | flops 1570483200 | bytes 6690820 | tf_op jit(solution)/shard_map/jr,jc->rc/dot_general | solution.py:89
  (65 shorter events, 50.0 us)
Async XLA Ops:
  7.2 72.5 %all-gather.9.cloned.1.call-start = ((), (), s32[]{:S(2)}) async-start(), calls=%async_computation.1 | async-start | bytes 4055040 | tf_op jit(solution)/shard_map/all_gather | solution.py:43
  11.7 133.8 %all-gather.11.cloned.1.call-start = ((), (), s32[]{:S(2)}) async-start(), calls=%async_computation.2 | async-start | bytes 4055040 | tf_op jit(solution)/shard_map/all_gather | solution.py:44
  15.8 193.8 %reduce-scatter.4.cloned.1.call-start = ((), (), s32[]{:S(2)}) async-start(), calls=%async_computation.9 | async-start | bytes 6082560
  154.2 132.8 %all-gather.13.cloned.1.call-start = ((), (), s32[]{:S(2)}) async-start(), calls=%async_computation.3 | async-start | bytes 3041280 | tf_op jit(solution)/shard_map/all_gather | solution.py:29
  254.3 69.0 %all-gather.15.cloned.1.call-start = ((), (), s32[]{:S(2)}) async-start(), calls=%async_computation.4 | async-start | bytes 3041280 | tf_op jit(solution)/shard_map/all_gather | solution.py:29
  254.4 11.1 %collective-permute-start = (bf16[264,528]{1,0:T(8,128)(2,1)}, bf16[264,528]{1,0:T(8,128)(2,1)S(1)}, u32[]{:S(2)}, u32[]{:S(2)}) collective-permute-start(bf16[264,528]{1,0:T(8,128)(2,1)} %get-tuple-element.16), channel_id=1, source_target_pairs={{0,8},{8,16},{16,24},{24,0},{1,9},{9,17},{17,25},{25,1},{2,10},{10... | collective-permute-start | bytes 836360 | tf_op jit(solution)/shard_map/ppermute | solution.py:19
  265.5 10.0 %collective-permute-start.1 = (bf16[264,528]{1,0:T(8,128)(2,1)S(1)}, bf16[264,528]{1,0:T(8,128)(2,1)S(1)}, u32[]{:S(2)}, u32[]{:S(2)}) collective-permute-start(bf16[264,528]{1,0:T(8,128)(2,1)S(1)} %collective-permute-done), channel_id=1, source_target_pairs={{0,8},{8,16},{16,24},{24,0},{1,9},{9,17},{17,25},{25,1},{2,10},{10... | collective-permute-start | bytes 836360 | tf_op jit(solution)/shard_map/ppermute | solution.py:19
  275.4 9.1 %collective-permute-start.2 = (bf16[264,528]{1,0:T(8,128)(2,1)S(1)}, bf16[264,528]{1,0:T(8,128)(2,1)S(1)}, u32[]{:S(2)}, u32[]{:S(2)}) collective-permute-start(bf16[264,528]{1,0:T(8,128)(2,1)S(1)} %collective-permute-done.1), channel_id=1, source_target_pairs={{0,8},{8,16},{16,24},{24,0},{1,9},{9,17},{17,25},{25,1},{2,10},{10... | collective-permute-start | bytes 836360 | tf_op jit(solution)/shard_map/ppermute | solution.py:19
  291.4 66.4 %all-gather.17.cloned.1.call-start = ((), (), s32[]{:S(2)}) async-start(), calls=%async_computation.5 | async-start | bytes 3041280 | tf_op jit(solution)/shard_map/all_gather | solution.py:29
  291.5 10.7 %collective-permute-start.3 = (bf16[264,528]{1,0:T(8,128)(2,1)S(1)}, bf16[264,528]{1,0:T(8,128)(2,1)S(1)}, u32[]{:S(2)}, u32[]{:S(2)}) collective-permute-start(bf16[264,528]{1,0:T(8,128)(2,1)S(1)} %get-tuple-element.15), channel_id=1, source_target_pairs={{0,8},{8,16},{16,24},{24,0},{1,9},{9,17},{17,25},{25,1},{2,10},{10... | collective-permute-start | bytes 836360 | tf_op jit(solution)/shard_map/ppermute | solution.py:19
  302.1 9.7 %collective-permute-start.4 = (bf16[264,528]{1,0:T(8,128)(2,1)S(1)}, bf16[264,528]{1,0:T(8,128)(2,1)S(1)}, u32[]{:S(2)}, u32[]{:S(2)}) collective-permute-start(bf16[264,528]{1,0:T(8,128)(2,1)S(1)} %collective-permute-done.3), channel_id=1, source_target_pairs={{0,8},{8,16},{16,24},{24,0},{1,9},{9,17},{17,25},{25,1},{2,10},{10... | collective-permute-start | bytes 836360 | tf_op jit(solution)/shard_map/ppermute | solution.py:19
  311.9 9.1 %collective-permute-start.5 = (bf16[264,528]{1,0:T(8,128)(2,1)S(1)}, bf16[264,528]{1,0:T(8,128)(2,1)}, u32[]{:S(2)}, u32[]{:S(2)}) collective-permute-start(bf16[264,528]{1,0:T(8,128)(2,1)S(1)} %collective-permute-done.4), channel_id=1, source_target_pairs={{0,8},{8,16},{16,24},{24,0},{1,9},{9,17},{17,25},{25,1},{2,10},{10... | collective-permute-start | bytes 836360 | tf_op jit(solution)/shard_map/ppermute | solution.py:19
  327.8 65.3 %all-gather.19.cloned.1.call-start = ((), (), s32[]{:S(2)}) async-start(), calls=%async_computation.6 | async-start | bytes 3041280 | tf_op jit(solution)/shard_map/all_gather | solution.py:29
  327.9 9.5 %collective-permute-start.12 = (bf16[264,528]{1,0:T(8,128)(2,1)}, bf16[264,528]{1,0:T(8,128)(2,1)S(1)}, u32[]{:S(2)}, u32[]{:S(2)}) collective-permute-start(bf16[264,528]{1,0:T(8,128)(2,1)} %get-tuple-element.14), channel_id=1, source_target_pairs={{0,8},{8,16},{16,24},{24,0},{1,9},{9,17},{17,25},{25,1},{2,10},{10... | collective-permute-start | bytes 836360 | tf_op jit(solution)/shard_map/ppermute | solution.py:19
  337.3 9.0 %collective-permute-start.13 = (bf16[264,528]{1,0:T(8,128)(2,1)S(1)}, bf16[264,528]{1,0:T(8,128)(2,1)S(1)}, u32[]{:S(2)}, u32[]{:S(2)}) collective-permute-start(bf16[264,528]{1,0:T(8,128)(2,1)S(1)} %collective-permute-done.12), channel_id=1, source_target_pairs={{0,8},{8,16},{16,24},{24,0},{1,9},{9,17},{17,25},{25,1},{2,10},{10... | collective-permute-start | bytes 836360 | tf_op jit(solution)/shard_map/ppermute | solution.py:19
  346.3 9.1 %collective-permute-start.14 = (bf16[264,528]{1,0:T(8,128)(2,1)S(1)}, bf16[264,528]{1,0:T(8,128)(2,1)}, u32[]{:S(2)}, u32[]{:S(2)}) collective-permute-start(bf16[264,528]{1,0:T(8,128)(2,1)S(1)} %collective-permute-done.13), channel_id=1, source_target_pairs={{0,8},{8,16},{16,24},{24,0},{1,9},{9,17},{17,25},{25,1},{2,10},{10... | collective-permute-start | bytes 836360 | tf_op jit(solution)/shard_map/ppermute | solution.py:19
  362.3 67.8 %all-gather.21.cloned.1.call-start = ((), (), s32[]{:S(2)}) async-start(), calls=%async_computation.7 | async-start | bytes 3041280 | tf_op jit(solution)/shard_map/all_gather | solution.py:29
  362.4 10.1 %collective-permute-start.9 = (bf16[264,528]{1,0:T(8,128)(2,1)S(1)}, bf16[264,528]{1,0:T(8,128)(2,1)S(1)}, u32[]{:S(2)}, u32[]{:S(2)}) collective-permute-start(bf16[264,528]{1,0:T(8,128)(2,1)S(1)} %get-tuple-element.13), channel_id=1, source_target_pairs={{0,8},{8,16},{16,24},{24,0},{1,9},{9,17},{17,25},{25,1},{2,10},{10... | collective-permute-start | bytes 836360 | tf_op jit(solution)/shard_map/ppermute | solution.py:19
  372.5 9.2 %collective-permute-start.10 = (bf16[264,528]{1,0:T(8,128)(2,1)S(1)}, bf16[264,528]{1,0:T(8,128)(2,1)S(1)}, u32[]{:S(2)}, u32[]{:S(2)}) collective-permute-start(bf16[264,528]{1,0:T(8,128)(2,1)S(1)} %collective-permute-done.9), channel_id=1, source_target_pairs={{0,8},{8,16},{16,24},{24,0},{1,9},{9,17},{17,25},{25,1},{2,10},{10... | collective-permute-start | bytes 836360 | tf_op jit(solution)/shard_map/ppermute | solution.py:19
  381.7 9.1 %collective-permute-start.11 = (bf16[264,528]{1,0:T(8,128)(2,1)S(1)}, bf16[264,528]{1,0:T(8,128)(2,1)}, u32[]{:S(2)}, u32[]{:S(2)}) collective-permute-start(bf16[264,528]{1,0:T(8,128)(2,1)S(1)} %collective-permute-done.10), channel_id=1, source_target_pairs={{0,8},{8,16},{16,24},{24,0},{1,9},{9,17},{17,25},{25,1},{2,10},{10... | collective-permute-start | bytes 836360 | tf_op jit(solution)/shard_map/ppermute | solution.py:19
  397.6 65.5 %all-gather.23.cloned.1.call-start = ((), (), s32[]{:S(2)}) async-start(), calls=%async_computation.8 | async-start | bytes 3041280 | tf_op jit(solution)/shard_map/all_gather | solution.py:85
  401.4 9.7 %collective-permute-start.6 = (bf16[264,528]{1,0:T(8,128)(2,1)S(1)}, bf16[264,528]{1,0:T(8,128)(2,1)S(1)}, u32[]{:S(2)}, u32[]{:S(2)}) collective-permute-start(bf16[264,528]{1,0:T(8,128)(2,1)S(1)} %convolution_convert_fusion.2), channel_id=1, source_target_pairs={{0,8},{8,16},{16,24},{24,0},{1,9},{9,17},{17,25},{25,1},{2,10},{10... | collective-permute-start | bytes 836360 | tf_op jit(solution)/shard_map/ppermute | solution.py:19
  411.1 9.1 %collective-permute-start.7 = (bf16[264,528]{1,0:T(8,128)(2,1)S(1)}, bf16[264,528]{1,0:T(8,128)(2,1)S(1)}, u32[]{:S(2)}, u32[]{:S(2)}) collective-permute-start(bf16[264,528]{1,0:T(8,128)(2,1)S(1)} %collective-permute-done.6), channel_id=1, source_target_pairs={{0,8},{8,16},{16,24},{24,0},{1,9},{9,17},{17,25},{25,1},{2,10},{10... | collective-permute-start | bytes 836360 | tf_op jit(solution)/shard_map/ppermute | solution.py:19
  420.2 9.0 %collective-permute-start.8 = (bf16[264,528]{1,0:T(8,128)(2,1)S(1)}, bf16[264,528]{1,0:T(8,128)(2,1)S(1)}, u32[]{:S(2)}, u32[]{:S(2)}) collective-permute-start(bf16[264,528]{1,0:T(8,128)(2,1)S(1)} %collective-permute-done.7), channel_id=1, source_target_pairs={{0,8},{8,16},{16,24},{24,0},{1,9},{9,17},{17,25},{25,1},{2,10},{10... | collective-permute-start | bytes 836360 | tf_op jit(solution)/shard_map/ppermute | solution.py:19
  (5 other events, 243.0 us)
Sparse Core Ops, SparseCore 0:
  11.8 67.7 all-gather.8
  81.8 63.6 all-gather.10
  154.3 55.2 reduce-scatter.3
  254.4 31.2 all-gather.12
  291.6 29.0 all-gather.14
  327.9 28.0 all-gather.16
  362.4 28.4 all-gather.18
  397.7 28.0 all-gather.20
  434.7 28.3 all-gather.22
